TPU v7x, 128 devices: a whole 4x4x4 slice. The times are simulated.
128 devices in a mesh: fs: 16 (over z, x), tp: 8 (over y, core).
Axes of the slice: x: 4, y: 4, z: 4, core: 2. Of those that a mesh axis runs over, the one named last changes fastest.
Arguments:
- saved_input: bfloat16 [49152, 2048], P('fs'), may hold values from -6 to 6
- proj_cot: bfloat16 [3, 49152, 2048], P(None, 'fs', 'tp'), may hold values from -0.02734375 to 0.02734375
- log_cache: float32 [16, 49152], P(None, 'fs'), as said below
- cache_cot: float32 [16, 49152], P(None, 'fs'), may hold values from -0.02734375 to 0.02734375
- proj_master: float32 [3, 2048, 2048], P(None, 'fs', 'tp'), may hold values from -0.125 to 0.125
- factors: bfloat16 [3, 2048, 256], P(None, 'fs'), may hold values from -0.125 to 0.125
- first_moment: float32 [3, 256, 2048], P(None, None, 'tp'), may hold values from -6 to 6
- second_moment: float32 [3, 256, 2048], P(None, None, 'tp'), may hold values from 0.01 to 10
- gate_master: float32 [16, 2048], replicated, may hold values from -0.125 to 0.125
- gate_first: float32 [16, 2048], replicated, may hold values from -6 to 6
- gate_second: float32 [16, 2048], replicated, may hold values from 0.1 to 3
Outputs:
- proj_step: float32 [3, 2048, 2048], P(None, 'fs', 'tp')
- proj_new: float32 [3, 2048, 2048], P(None, 'fs', 'tp')
- proj_copy: bfloat16 [3, 2048, 2048], P(None, None, 'tp')
- first_new: float32 [3, 256, 2048], P(None, None, 'tp')
- second_new: float32 [3, 256, 2048], P(None, None, 'tp')
- gate_new: float32 [16, 2048], replicated
- gate_copy: bfloat16 [16, 2048], replicated
- gate_first_new: float32 [16, 2048], replicated
- gate_second_new: float32 [16, 2048], replicated
Inputs may be any that keep to these rules, and one draw needn't show every extreme that they name: `log_cache`: each head's values never rise along positions.
All inputs are finite; a program needn't handle non-finite values.
Results may differ from a plain program's by a relative error of at most 0.0004.
Values may be sent and summed in bfloat16 or wider, within the bound.
No kernel may reach another device: no remote copies, remote signals or barrier semaphores. Data moves between devices by JAX's collectives and lax.ppermute only.
A program may use at most 128 MiB of HBM per device.

v0:
```python
import jax
import jax.numpy as jnp
from jax import lax
from jax.sharding import PartitionSpec as P

BETA_ONE = 0.8
BETA_TWO = 0.9
LEARN = 0.001


def from_behind(x, axis, by):
    peers = lax.axis_size(axis)
    pairs = [(i, i + by) for i in range(peers) if 0 <= i + by < peers]
    return lax.ppermute(x, axis, pairs)


def from_everyone(x, axis):
    copies = jnp.broadcast_to(x, (lax.axis_size(axis), *x.shape))
    return lax.all_to_all(copies, axis, split_axis=0, concat_axis=0, tiled=True)


def folded_in_pairs(pieces, combine):
    while len(jax.tree.leaves(pieces)[0]) > 1:
        pieces = jax.vmap(combine)(*(pieces[side::2] for side in (0, 1)))
    return pieces[0]


def carried_in(x, axis, combine, identity):
    peers, place = (lax.axis_size(axis), lax.axis_index(axis))
    passed = jnp.arange(peers) > place

    def kept(part, zero, own):
        part = jnp.where(
            passed.reshape(-1, *(1 for _ in own.shape)), part, jnp.asarray(zero, own.dtype)
        )
        return part[::-1]

    pieces = from_everyone(x, axis)
    return folded_in_pairs(kept(pieces, identity, x), combine)


def rows_for(lines, peers):
    spare = -lines.shape[0] % peers
    if not spare:
        return lines
    return jnp.concatenate([lines, jnp.zeros((spare, *lines.shape[1:]), lines.dtype)])


def in_order(parts, dim):
    parts = jnp.moveaxis(parts, 0, dim)
    lengths = parts.shape
    return parts.reshape(*lengths[:dim], lengths[dim] * lengths[dim + 1], *lengths[dim + 2 :])


def collect(x, axis, dim):
    return in_order(from_everyone(x, axis), dim)


def cut_along(x, dim, peers):
    lengths = x.shape
    parts = x.reshape(*lengths[:dim], peers, lengths[dim] // peers, *lengths[dim + 1 :])
    return jnp.moveaxis(parts, dim, 0)


def summed_on_arrival(x, axis, dim):
    parts = cut_along(x, dim, lax.axis_size(axis))
    arrived = lax.all_to_all(parts, axis, split_axis=0, concat_axis=0, tiled=True)
    return arrived.sum(axis=0)


def total_of(x, axes):
    padded = rows_for(x, lax.axis_size(axes))
    whole = collect(summed_on_arrival(padded, axes, 0), axes, 0)
    return lax.slice_in_dim(whole, 0, len(x)).reshape(x.shape)


def in_one(arrays, axis):
    ravelled, at, finished = (jnp.concatenate([a.reshape(-1) for a in arrays]), 0, [])
    so_far = total_of(ravelled, axis)
    for a in arrays:
        finished.append(so_far[at : at + a.size].reshape(a.shape))
        at += a.size
    return tuple(finished)


def over_copies(x, axis):
    everything = from_everyone(x, axis)
    return jnp.sum(everything, axis=0)


def add_pair(earlier, later_part):
    return earlier + later_part


def local(
    saved_input,
    proj_cot,
    log_cache,
    cache_cot,
    proj_master,
    factors,
    first_moment,
    second_moment,
    gate_master,
    gate_first,
    gate_second,
):
    heads = log_cache.shape[0]
    edge = from_behind(log_cache[:, -1:], "fs", 1)
    previous = jnp.concatenate([edge, log_cache[:, :-1]], axis=1)
    gate_logarithm = log_cache - previous
    carried = carried_in(
        jnp.sum(cache_cot, axis=1), "fs", add_pair, jnp.zeros((heads,), jnp.float32)
    )
    later = jnp.flip(jnp.cumsum(jnp.flip(cache_cot, 1), axis=1), 1) + carried[:, None]
    gate_cot = (later * -jnp.expm1(gate_logarithm)).astype(jnp.bfloat16)
    gate_part = jnp.dot(gate_cot, saved_input, preferred_element_type=jnp.float32)
    all_factors = lax.all_gather(factors, "fs", axis=1, tiled=True)
    reduced = jnp.einsum(
        "td,rdk->rtk", saved_input, all_factors, preferred_element_type=jnp.float32
    )
    upper_half = lax.optimization_barrier(reduced.astype(jnp.bfloat16))
    lower_half = (reduced - upper_half.astype(jnp.float32)).astype(jnp.bfloat16)
    low_part = jnp.einsum("rtk,rtw->rkw", upper_half, proj_cot, preferred_element_type=jnp.float32)
    low_part = low_part + jnp.einsum(
        "rtk,rtw->rkw", lower_half, proj_cot, preferred_element_type=jnp.float32
    )
    low, gate_grad = in_one((low_part, gate_part), "fs")
    first_new = BETA_ONE * first_moment + (1.0 - BETA_ONE) * low
    second_new = BETA_TWO * second_moment + (1.0 - BETA_TWO) * low * low
    direction = first_new / jnp.sqrt(second_new)
    squares = over_copies(jnp.sum(direction * direction), "tp")
    entries = direction.shape[0] * direction.shape[1] * direction.shape[2] * lax.axis_size("tp")
    scale = lax.rsqrt(squares / entries + 1e-06)
    product = jnp.einsum(
        "rdk,rkw->rdw", factors.astype(jnp.float32), direction, precision=lax.Precision.HIGHEST
    )
    proj_step = scale * product
    proj_new = proj_master - LEARN * proj_step
    proj_copy = lax.all_gather(proj_new.astype(jnp.bfloat16), "fs", axis=1, tiled=True)
    gate_first_new = BETA_ONE * gate_first + (1.0 - BETA_ONE) * gate_grad
    gate_second_new = BETA_TWO * gate_second + (1.0 - BETA_TWO) * gate_grad * gate_grad
    gate_new = gate_master - LEARN * gate_first_new / jnp.sqrt(gate_second_new)
    gate_copy = gate_new.astype(jnp.bfloat16)
    return (
        proj_step,
        proj_new,
        proj_copy,
        first_new,
        second_new,
        gate_new,
        gate_copy,
        gate_first_new,
        gate_second_new,
    )


def solution(mesh):
    placed = (
        P("fs", None),
        P(None, "fs", "tp"),
        P(None, "fs"),
        P(None, "fs"),
        P(None, "fs", "tp"),
        P(None, "fs", None),
        P(None, None, "tp"),
        P(None, None, "tp"),
        P(),
        P(),
        P(),
    )
    return jax.shard_map(
        local,
        mesh=mesh,
        in_specs=placed,
        out_specs=(
            P(None, "fs", "tp"),
            P(None, "fs", "tp"),
            P(None, None, "tp"),
            P(None, None, "tp"),
            P(None, None, "tp"),
            P(),
            P(),
            P(),
            P(),
        ),
        check_vma=False,
    )
```

profile of v0, /device:TPU:0, one launch (start us, length us, event | category | flops | bytes accessed | tf_op | source)
XLA Modules:
  0.0 206.4 jit_solution(16304343146461172091)
XLA Ops:
  7.2 0.0 all-gather.3.cloned.1.call-start
  7.2 1.7 copy.44
  9.0 0.0 all-gather.3.cloned.1.call-update
  9.0 1.1 reduce_sum.36
  10.1 0.6 broadcast_in_dim.22
  10.7 8.0 %all-to-all-start = ((f32[16,1,16]{2,1,0:T(1,128)}), f32[16,1,16]{2,1,0:T(1,128)S(1)}, u32[]{:S(2)}, u32[]{:S(2)}) async-start(f32[16,1,16]{2,1,0:T(1,128)} %broadcast_in_dim.22), calls=%async_computation | async-start | bytes 16384 | tf_op jit(solution)/shard_map/all_to_all | solution.py:19
  18.7 0.8 slice.65
  19.4 3.8 %collective-permute-start = (f32[16,1]{1,0:T(8,128)S(1)}, f32[16,1]{1,0:T(8,128)S(1)}, u32[]{:S(2)}, u32[]{:S(2)}) collective-permute-start(f32[16,1]{1,0:T(8,128)S(1)} %slice.65), channel_id=1, source_target_pairs={{0,8},{8,16},{16,24},{24,32},{32,40},{40,48},{48,56},{56,64},{64,7... | collective-permute-start | bytes 200 | tf_op jit(solution)/shard_map/ppermute | solution.py:14
  23.3 9.3 %rev.8 = f32[16,3072]{1,0:T(8,128)S(1)} reverse(f32[16,3072]{1,0:T(8,128)} %param.14), dimensions={1} | reverse | bytes 393216 | tf_op jit(solution)/shard_map/jit(_flip)/rev | solution.py:115
  32.6 4.6 %reduce-window.6 = f32[16,24,128]{2,1,0:T(8,128)S(1)} reduce-window(f32[16,24,128]{2,1,0:T(8,128)S(1)} %bitcast.46, f32[]{:T(128)} %constant.11.clone.1), window={size=1x1x128 pad=0_0x0_0x127_0}, to_apply=%region_0.0 | reduce-window | flops 6242304 | bytes 393220 | tf_op jit(solution)/shard_map/reduce-window
  37.3 0.2 slice_reduce_fusion
  37.5 0.2 reduce-window.9
  37.7 0.1 broadcast_add_fusion
  37.8 1.8 rev.9
  39.6 0.0 all-to-all-done
  39.6 0.1 broadcast_select_fusion
  39.9 0.0 collective-permute-done
  39.9 6.6 %convolution_bitcast_fusion = f32[2,16,8,128]{3,2,1,0:T(8,128)S(1)} fusion(bf16[3072,2048]{1,0:T(8,128)(2,1)} %param.11, f32[16,3072]{1,0:T(8,128)} %param.13, f32[16,3071]{1,0:T(8,128)} %bitcast.43, f32[16,1]{1,0:T(8,128)S(1)} %collective-permute-done, f32[16,3072]{1,0:T(8,128)S(1)} %rev.9, f32[16]{0:T(128)S(1)} %add_bitcast_fusion), kind=kOutput, calls=%fused_computation.10 | convolution fusion | flops 201621504 | bytes 13303872 | tf_op jit(solution)/shard_map/dot_general | solution.py:117
  46.5 18.7 %all-gather.3.cloned.1.call-done = bf16[3,2048,256]{1,2,0:T(8,128)(2,1)} async-done(((bf16[3,128,256]{1,2,0:T(8,128)(2,1)}), bf16[3,2048,256]{1,2,0:T(8,128)(2,1)}) %all-gather.3.cloned.1.call-update) | async-done | bytes 3145744 | tf_op jit(solution)/shard_map/all_gather | solution.py:118
  65.3 16.1 %bitcast_convert_fusion = (bf16[3,3072,256]{1,2,0:T(8,128)(2,1)S(1)}, f32[3,256,3072]{2,1,0:T(8,128)}) fusion(bf16[3,2048,256]{1,2,0:T(8,128)(2,1)} %all-gather.3.cloned.1.call-done, bf16[3072,2048]{1,0:T(8,128)(2,1)} %param.11), kind=kOutput, calls=%fused_computation.3 | convolution fusion | flops 9666035712 | bytes 29884416 | tf_op jit(solution)/shard_map/td,rdk->rtk/dot_general | solution.py:119
  81.4 3.7 %fusion.22 = f32[3,256,256]{2,1,0:T(8,128)S(1)} fusion(bf16[3,3072,256]{1,2,0:T(8,128)(2,1)S(1)} %get-tuple-element.63, bf16[3,3072,256]{2,1,0:T(8,128)(2,1)} %param.12), kind=kOutput, calls=%fused_computation.36 | convolution fusion | flops 1207959552 | bytes 10223616 | tf_op jit(solution)/shard_map/rtk,rtw->rkw/dot_general | solution.py:124
  85.1 6.4 %fusion.5 = f32[3,256,256]{2,1,0:T(8,128)S(1)} fusion(f32[3,256,256]{2,1,0:T(8,128)S(1)} %fusion.22, bf16[3,3072,256]{2,1,0:T(8,128)(2,1)} %param.12, f32[3,256,3072]{2,1,0:T(8,128)} %get-tuple-element.64, bf16[3,3072,256]{1,2,0:T(8,128)(2,1)S(1)} %get-tuple-element.63), kind=kOutput, calls=%fused_computation.6 | convolution fusion | flops 1215234048 | bytes 20447232 | tf_op jit(solution)/shard_map/rtk,rtw->rkw/dot_general | solution.py:125
  91.5 0.0 copy-start.3
  91.5 0.4 copy.55
  91.9 0.1 pad_maximum_fusion
  92.0 19.2 %all_to_all.30 = f32[16,1,14336]{2,1,0:T(1,128)S(1)} all-to-all(f32[16,1,14336]{2,1,0:T(1,128)S(1)} %bitcast.40), channel_id=1, replica_groups=mesh['fs'=16,'tp'=8] {'fs'}, dimensions={0} | all-to-all | bytes 1835008 | tf_op jit(solution)/shard_map/all_to_all | solution.py:67
  111.2 0.6 reduce_sum.37
  111.8 1.4 broadcast_in_dim.24
  113.2 3.8 %all-to-all-start.2 = ((f32[16,1,14336]{2,1,0:T(1,128)}), f32[16,1,14336]{2,1,0:T(1,128)S(1)}, u32[]{:S(2)}, u32[]{:S(2)}) async-start(f32[16,1,14336]{2,1,0:T(1,128)} %broadcast_in_dim.24), calls=%async_computation.2 | async-start | bytes 1835008 | tf_op jit(solution)/shard_map/all_to_all | solution.py:19
  117.0 0.2 all-gather.5.cloned.1.call-start
  117.2 0.0 copy-done.3
  117.2 0.9 copy.48
  118.1 12.4 %all-to-all-done.2 = f32[16,1,14336]{2,1,0:T(1,128)S(1)} async-done(((f32[16,1,14336]{2,1,0:T(1,128)}), f32[16,1,14336]{2,1,0:T(1,128)S(1)}, u32[]{:S(2)}, u32[]{:S(2)}) %all-to-all-start.2) | async-done | bytes 917536 | tf_op jit(solution)/shard_map/all_to_all | solution.py:19
  130.5 0.1 slice.72
  130.6 0.2 reshape.69
  130.8 2.3 %multiply_reduce_fusion = (f32[]{:T(128)}, f32[3,256,256]{2,1,0:T(8,128)S(1)}, f32[3,256,256]{2,1,0:T(8,128)S(1)}) fusion(f32[3,256,256]{2,1,0:T(8,128)S(1)} %reshape.69, f32[3,256,256]{2,1,0:T(8,128)} %param.18, f32[3,256,256]{2,1,0:T(8,128)} %param.17), kind=kLoop, calls=%fused_computation.13 | loop fusion | flops 1966079 | bytes 3932164 | tf_op jit(solution)/shard_map/reduce_sum | solution.py:132
  133.1 0.7 broadcast_in_dim.25
  133.8 9.4 %all_to_all.31 = f32[8,1,1]{2,1,0:T(1,128)S(1)} all-to-all(f32[8,1,1]{2,1,0:T(1,128)S(1)} %broadcast_in_dim.25), channel_id=1, replica_groups=mesh['fs'=16,'tp'=8] {'tp'}, dimensions={0} | all-to-all | bytes 64 | tf_op jit(solution)/shard_map/all_to_all | solution.py:19
  143.2 0.6 reduce_sum.39
  144.5 2.7 %fusion.20 = (bf16[3,128,256]{1,2,0:T(8,128)(2,1)}, f32[3,128,256]{1,2,0:T(8,128)S(1)}, f32[3,128,256]{1,2,0:T(8,128)}) fusion(f32[3,128,256]{1,2,0:T(8,128)} %copy.48, bf16[3,128,256]{2,1,0:T(8,128)(2,1)S(1)} %copy-done.2, f32[3,256,256]{2,1,0:T(8,128)S(1)} %get-tuple-element.62, f32[3,256,256]{2,1,0:T(8,128)S(1)} %get-tuple-element.61, f32[]{:T(128)S(6)} %rsqrt.5), kind=kOutput, calls=%fused_computation.35 | convolution fusion | flops 302579712 | bytes 3145732 | tf_op jit(solution)/shard_map/rdk,rkw->rdw/dot_general | solution.py:135
  147.1 0.0 all-gather.5.cloned.1.call-update
  147.2 2.2 %reduce.3 = f32[16,14336]{1,0:T(8,128)S(1)} reduce(f32[16,1,14336]{2,1,0:T(1,128)S(1)} %all-to-all-done.2, f32[]{:T(128)} %constant.8), dimensions={1}, to_apply=%all_to_all.24.reduce_sub_computation | reduce | bytes 1835012 | tf_op jit(solution)/shard_map/all_to_all | solution.py:19
  149.4 0.1 slice.68
  149.5 1.7 fusion.18
  151.2 1.9 copy.49
  153.1 0.9 copy.50
  154.1 40.8 %all-gather.5.cloned.1.call-done = bf16[3,2048,256]{1,2,0:T(8,128)(2,1)} async-done(((bf16[3,128,256]{1,2,0:T(8,128)(2,1)}), bf16[3,2048,256]{1,2,0:T(8,128)(2,1)}) %all-gather.5.cloned.1.call-update) | async-done | bytes 3145744 | tf_op jit(solution)/shard_map/all_gather | solution.py:140
  194.9 4.6 %copy.51 = bf16[3,2048,256]{2,1,0:T(8,128)(2,1)} copy(bf16[3,2048,256]{1,2,0:T(8,128)(2,1)} %all-gather.5.cloned.1.call-done) | data formatting | bytes 6291456
  (26 shorter events, 0.3 us)
Async XLA Ops:
  7.2 58.1 %all-gather.3.cloned.1.call-start = ((), (), s32[]{:S(2)}) async-start(), calls=%async_computation.4 | async-start | bytes 3342336 | tf_op jit(solution)/shard_map/all_gather | solution.py:118
  10.7 28.9 %all-to-all-start = ((f32[16,1,16]{2,1,0:T(1,128)}), f32[16,1,16]{2,1,0:T(1,128)S(1)}, u32[]{:S(2)}, u32[]{:S(2)}) async-start(f32[16,1,16]{2,1,0:T(1,128)} %broadcast_in_dim.22), calls=%async_computation | async-start | bytes 16384 | tf_op jit(solution)/shard_map/all_to_all | solution.py:19
  19.4 20.4 %collective-permute-start = (f32[16,1]{1,0:T(8,128)S(1)}, f32[16,1]{1,0:T(8,128)S(1)}, u32[]{:S(2)}, u32[]{:S(2)}) collective-permute-start(f32[16,1]{1,0:T(8,128)S(1)} %slice.65), channel_id=1, source_target_pairs={{0,8},{8,16},{16,24},{24,32},{32,40},{40,48},{48,56},{56,64},{64,7... | collective-permute-start | bytes 200 | tf_op jit(solution)/shard_map/ppermute | solution.py:14
  91.5 25.7 %copy-start.3 = (f32[3,128,256]{2,1,0:T(8,128)S(1)}, f32[3,128,256]{2,1,0:T(8,128)}, u32[]{:S(2)}) copy-start(f32[3,128,256]{2,1,0:T(8,128)} %param.15) | copy-start | bytes 1179652
  113.2 31.3 %copy-start.2 = (bf16[3,128,256]{2,1,0:T(8,128)(2,1)S(1)}, bf16[3,128,256]{2,1,0:T(8,128)(2,1)}, u32[]{:S(2)}) copy-start(bf16[3,128,256]{2,1,0:T(8,128)(2,1)} %param.16) | copy-start | bytes 589828
  113.2 17.3 %all-to-all-start.2 = ((f32[16,1,14336]{2,1,0:T(1,128)}), f32[16,1,14336]{2,1,0:T(1,128)S(1)}, u32[]{:S(2)}, u32[]{:S(2)}) async-start(f32[16,1,14336]{2,1,0:T(1,128)} %broadcast_in_dim.24), calls=%async_computation.2 | async-start | bytes 1835008 | tf_op jit(solution)/shard_map/all_to_all | solution.py:19
  117.0 77.9 %all-gather.5.cloned.1.call-start = ((), (), s32[]{:S(2)}) async-start(), calls=%async_computation.5 | async-start | bytes 3342336 | tf_op jit(solution)/shard_map/all_gather | solution.py:140
  133.1 14.1 %copy-start.1 = (f32[3,256,256]{2,1,0:T(8,128)}, f32[3,256,256]{2,1,0:T(8,128)S(1)}, u32[]{:S(2)}) copy-start(f32[3,256,256]{2,1,0:T(8,128)S(1)} %get-tuple-element.62) | copy-start | bytes 2359300
  133.1 21.0 %copy-start = (f32[3,256,256]{2,1,0:T(8,128)}, f32[3,256,256]{2,1,0:T(8,128)S(1)}, u32[]{:S(2)}) copy-start(f32[3,256,256]{2,1,0:T(8,128)S(1)} %get-tuple-element.61) | copy-start | bytes 2359300
  133.1 16.5 %copy-start.4 = (f32[16,2048]{1,0:T(8,128)S(1)}, f32[16,2048]{1,0:T(8,128)}, u32[]{:S(2)}) copy-start(f32[16,2048]{1,0:T(8,128)} %param.19) | copy-start | bytes 393220
  133.1 16.5 %copy-start.5 = (f32[16,2048]{1,0:T(8,128)S(1)}, f32[16,2048]{1,0:T(8,128)}, u32[]{:S(2)}) copy-start(f32[16,2048]{1,0:T(8,128)} %param.20) | copy-start | bytes 393220
Sparse Core Ops, SparseCore 0:
  10.7 54.5 all-gather.2
  147.3 47.5 all-gather.4
where the time goes:
time: 208 us; the launch traced here: 206 us
  waiting for transfers between devices  72 us (35%)
  matrix products  35.5 us (17%)
  blocking collectives  28.6 us (14%)
  local copies, waits for them, and re-layouts  26.1 us (13%)
  starting transfers between devices  15.8 us (8%)
  between operations  14.9 us (7%)
  other arithmetic  13.5 us (6%)
    all_gather x1, waiting for transfers between devices, local(): lax.all_gather(proj_new.astype(jnp.bfloat16), 'fs', axis=1, tiled=True)  40.8 us
    all_to_all x1, blocking collectives, summed_on_arrival(): lax.all_to_all(parts, axis, split_axis=0, concat_axis=0, tiled=True)  19.2 us
    all_gather x1, waiting for transfers between devices, local(): all_factors = lax.all_gather(factors, 'fs', axis=1, tiled=True)  18.7 us
    dot_general x1, matrix products, local(): jnp.einsum('td,rdk->rtk', saved_input, all_factors, preferred_element_typ...  16.1 us
    all_to_all x2, waiting for transfers between devices, from_everyone(): return lax.all_to_all(copies, axis, split_axis=0, concat_axis=0, tiled=True)  12.4 us
    all_to_all x2, starting transfers between devices, from_everyone(): return lax.all_to_all(copies, axis, split_axis=0, concat_axis=0, tiled=True)  11.8 us
    unnamed x21, local copies, waits for them, and re-layouts  10.7 us
    all_to_all x1, blocking collectives, from_everyone(): return lax.all_to_all(copies, axis, split_axis=0, concat_axis=0, tiled=True)  9.37 us
  transfers between devices with their start and end apart: 5, of which 3 were waited for; matrix products, arithmetic and copies ran while one was open for 16% of the time, Pallas kernels for 0%

commit v1 on v0

--- a/solution.py
+++ b/solution.py
@@ -115,7 +115,9 @@
     later = jnp.flip(jnp.cumsum(jnp.flip(cache_cot, 1), axis=1), 1) + carried[:, None]
     gate_cot = (later * -jnp.expm1(gate_logarithm)).astype(jnp.bfloat16)
     gate_part = jnp.dot(gate_cot, saved_input, preferred_element_type=jnp.float32)
-    all_factors = lax.all_gather(factors, "fs", axis=1, tiled=True)
+    all_factors = jnp.concatenate(
+        lax.all_to_all(jnp.stack([factors] * lax.axis_size("fs")), "fs", 0, 0), axis=1
+    )
     reduced = jnp.einsum(
         "td,rdk->rtk", saved_input, all_factors, preferred_element_type=jnp.float32
     )

time: 208 us -> 222 us (1.067)
  local copies, waits for them, and re-layouts: 26.1 us -> 36.3 us
  waiting for transfers between devices: 72 us -> 63 us
  blocking collectives: 28.6 us -> 33.5 us
  other arithmetic: 13.5 us -> 17.7 us
  starting transfers between devices: 15.8 us -> 20 us
    all_gather x1 -> x0, waiting for transfers between devices: 18.7 us -> none  [local(): all_factors = lax.all_gather(factors, 'fs', axis=1, tiled=True)]
    rev x1, local copies, waits for them, and re-layouts: 1.75 us -> 9.32 us  [local(): jnp.flip(jnp.cumsum(jnp.flip(cache_cot, 1), axis=1), 1) + carried[:, None]]
    all_to_all x2, waiting for transfers between devices: 12.4 us -> 18.6 us  [from_everyone(): return lax.all_to_all(copies, axis, split_axis=0, concat_axis=0, tiled=True)]
    all_to_all x1, blocking collectives: 19.2 us -> 23.9 us  [summed_on_arrival(): lax.all_to_all(parts, axis, split_axis=0, concat_axis=0, tiled=True)]
    all_to_all x0 -> x1, starting transfers between devices: none -> 3.74 us  [local(): lax.all_to_all(jnp.stack([factors] * lax.axis_size('fs')), 'fs', 0, 0)]
    another operation x3, other arithmetic: 4.9 us -> 8.48 us
    ppermute x1, waiting for transfers between devices: 0.01 us -> 3.5 us  [from_behind(): return lax.ppermute(x, axis, pairs)]
    another operation x0 -> x1, local copies, waits for them, and re-layouts: none -> 2.41 us  [local(): jnp.stack([factors] * lax.axis_size('fs'))]
  transfers between devices with their start and end apart: 5 -> 5, of which waited for: 3 -> 4; matrix products, arithmetic and copies ran while one was open for 16% -> 21% of each run, Pallas kernels for 0% -> 0%
where the time goes in v1:
time: 222 us; the launch traced here: 220 us
  waiting for transfers between devices  63 us (28%)
  local copies, waits for them, and re-layouts  36.3 us (16%)
  matrix products  34.7 us (16%)
  blocking collectives  33.5 us (15%)
  starting transfers between devices  20 us (9%)
  other arithmetic  17.7 us (8%)
  between operations  14.9 us (7%)
    all_gather x1, waiting for transfers between devices, local(): lax.all_gather(proj_new.astype(jnp.bfloat16), 'fs', axis=1, tiled=True)  40.8 us
    all_to_all x1, blocking collectives, summed_on_arrival(): lax.all_to_all(parts, axis, split_axis=0, concat_axis=0, tiled=True)  23.9 us
    all_to_all x2, waiting for transfers between devices, from_everyone(): return lax.all_to_all(copies, axis, split_axis=0, concat_axis=0, tiled=True)  18.6 us
    dot_general x1, matrix products, local(): jnp.einsum('td,rdk->rtk', saved_input, all_factors, preferred_element_typ...  15.2 us
    unnamed x27, local copies, waits for them, and re-layouts  12.3 us
    all_to_all x2, starting transfers between devices, from_everyone(): return lax.all_to_all(copies, axis, split_axis=0, concat_axis=0, tiled=True)  11.9 us
    all_to_all x1, blocking collectives, from_everyone(): return lax.all_to_all(copies, axis, split_axis=0, concat_axis=0, tiled=True)  9.57 us
    rev x1, local copies, waits for them, and re-layouts, local(): jnp.flip(jnp.cumsum(jnp.flip(cache_cot, 1), axis=1), 1) + carried[:, None]  9.32 us
  transfers between devices with their start and end apart: 5, of which 4 were waited for; matrix products, arithmetic and copies ran while one was open for 21% of the time, Pallas kernels for 0%

profile of v1, /device:TPU:0, one launch (start us, length us, event | category | flops | bytes accessed | tf_op | source)
XLA Modules:
  0.0 220.1 jit_solution(15955152238033543435)
XLA Ops:
  7.2 1.1 reduce_sum.36
  8.2 0.6 broadcast_in_dim.22
  8.8 8.0 %all-to-all-start.1 = ((f32[16,1,16]{2,1,0:T(1,128)}), f32[16,1,16]{2,1,0:T(1,128)S(1)}, u32[]{:S(2)}, u32[]{:S(2)}) async-start(f32[16,1,16]{2,1,0:T(1,128)} %broadcast_in_dim.22), calls=%async_computation.1 | async-start | bytes 16384 | tf_op jit(solution)/shard_map/all_to_all | solution.py:19
  16.8 1.1 copy.46
  18.0 0.0 copy-start.3
  18.0 6.4 %all-to-all-done.1 = f32[16,1,16]{2,1,0:T(1,128)S(1)} async-done(((f32[16,1,16]{2,1,0:T(1,128)}), f32[16,1,16]{2,1,0:T(1,128)S(1)}, u32[]{:S(2)}, u32[]{:S(2)}) %all-to-all-start.1) | async-done | bytes 1056 | tf_op jit(solution)/shard_map/all_to_all | solution.py:19
  24.4 2.4 %stack.2 = bf16[16,3,128,256]{2,3,1,0:T(8,128)(2,1)} broadcast(bf16[3,128,256]{1,2,0:T(8,128)(2,1)S(1)} %copy.46), dimensions={1,2,3} | broadcast | bytes 3342336 | tf_op jit(solution)/shard_map/stack | solution.py:119
  26.8 3.7 %all-to-all-start = ((bf16[16,3,128,256]{2,3,1,0:T(8,128)(2,1)}), bf16[16,3,128,256]{2,3,1,0:T(8,128)(2,1)S(1)}, u32[]{:S(2)}, u32[]{:S(2)}) async-start(bf16[16,3,128,256]{2,3,1,0:T(8,128)(2,1)} %stack.2), calls=%async_computation | async-start | bytes 6291456 | tf_op jit(solution)/shard_map/all_to_all | solution.py:119
  30.5 0.7 slice.65
  31.2 4.3 %collective-permute-start = (f32[16,1]{1,0:T(8,128)}, f32[16,1]{1,0:T(8,128)}, u32[]{:S(2)}, u32[]{:S(2)}) collective-permute-start(f32[16,1]{1,0:T(8,128)} %slice.65), channel_id=1, source_target_pairs={{0,8},{8,16},{16,24},{24,32},{32,40},{40,48},{48,56},{56,64},{64,7... | collective-permute-start | bytes 200 | tf_op jit(solution)/shard_map/ppermute | solution.py:14
  35.5 8.1 %rev.8 = f32[16,3072]{1,0:T(8,128)} reverse(f32[16,3072]{1,0:T(8,128)S(1)} %copy-done.3), dimensions={1} | reverse | bytes 393216 | tf_op jit(solution)/shard_map/jit(_flip)/rev | solution.py:115
  43.6 1.6 copy.60
  45.2 8.2 %reduce-window.6 = f32[16,24,128]{2,1,0:T(8,128)S(1)} reduce-window(f32[16,24,128]{2,1,0:T(8,128)} %bitcast.55, f32[]{:T(128)} %constant.11.clone.1), window={size=1x1x128 pad=0_0x0_0x127_0}, to_apply=%region_0.0 | reduce-window | flops 6242304 | bytes 393220 | tf_op jit(solution)/shard_map/reduce-window
  53.4 0.2 slice_reduce_fusion
  53.7 0.2 reduce-window.9
  53.8 0.1 broadcast_add_fusion
  54.0 0.7 copy.70
  54.7 9.3 %rev.9 = f32[16,3072]{1,0:T(8,128)S(1)} reverse(f32[16,3072]{1,0:T(8,128)} %bitcast.56), dimensions={1} | reverse | bytes 393216 | tf_op jit(solution)/shard_map/jit(_flip)/rev | solution.py:115
  64.0 0.8 broadcast_select_fusion
  65.0 3.5 %collective-permute-done = f32[16,1]{1,0:T(8,128)} collective-permute-done((f32[16,1]{1,0:T(8,128)}, f32[16,1]{1,0:T(8,128)}, u32[]{:S(2)}, u32[]{:S(2)}) %collective-permute-start) | collective-permute-done | bytes 96 | tf_op jit(solution)/shard_map/ppermute | solution.py:14
  68.5 6.4 %convolution_bitcast_fusion = f32[2,16,8,128]{3,2,1,0:T(8,128)S(1)} fusion(bf16[3072,2048]{1,0:T(8,128)(2,1)} %param.11, f32[16,3072]{1,0:T(8,128)S(1)} %copy-done.2, f32[16,3071]{1,0:T(8,128)S(1)} %bitcast.52, f32[16,1]{1,0:T(8,128)} %collective-permute-done, f32[16,3072]{1,0:T(8,128)S(1)} %rev.9, f32[16]{0:T(128)S(1)} %add_bitcast_fusion), kind=kOutput, calls=%fused_computation.12 | convolution fusion | flops 201621504 | bytes 13303872 | tf_op jit(solution)/shard_map/dot_general | solution.py:117
  74.9 15.2 %bitcast_convert_fusion = (bf16[3,3072,256]{1,2,0:T(8,128)(2,1)S(1)}, f32[3,256,3072]{2,1,0:T(8,128)}) fusion(bf16[3072,2048]{1,0:T(8,128)(2,1)} %param.11, bf16[16,3,128,256]{2,3,1,0:T(8,128)(2,1)S(1)} %all-to-all-done), kind=kOutput, calls=%fused_computation.3 | convolution fusion | flops 9666035712 | bytes 29884416 | tf_op jit(solution)/shard_map/td,rdk->rtk/dot_general | solution.py:121
  90.1 3.8 %fusion.24 = f32[3,256,256]{2,1,0:T(8,128)S(1)} fusion(bf16[3,3072,256]{1,2,0:T(8,128)(2,1)S(1)} %get-tuple-element.63, bf16[3,3072,256]{2,1,0:T(8,128)(2,1)} %param.12), kind=kOutput, calls=%fused_computation.38 | convolution fusion | flops 1207959552 | bytes 10223616 | tf_op jit(solution)/shard_map/rtk,rtw->rkw/dot_general | solution.py:126
  93.8 6.7 %fusion.7 = f32[3,256,256]{2,1,0:T(8,128)S(1)} fusion(f32[3,256,256]{2,1,0:T(8,128)S(1)} %fusion.24, bf16[3,3072,256]{2,1,0:T(8,128)(2,1)} %param.12, f32[3,256,3072]{2,1,0:T(8,128)} %get-tuple-element.64, bf16[3,3072,256]{1,2,0:T(8,128)(2,1)S(1)} %get-tuple-element.63), kind=kOutput, calls=%fused_computation.8 | convolution fusion | flops 1215234048 | bytes 20447232 | tf_op jit(solution)/shard_map/rtk,rtw->rkw/dot_general | solution.py:127
  100.5 0.4 copy.59
  100.9 0.1 pad_maximum_fusion
  101.0 23.9 %all_to_all.35 = f32[16,1,14336]{2,1,0:T(1,128)S(1)} all-to-all(f32[16,1,14336]{2,1,0:T(1,128)S(1)} %bitcast.49), channel_id=1, replica_groups=mesh['fs'=16,'tp'=8] {'fs'}, dimensions={0} | all-to-all | bytes 1835008 | tf_op jit(solution)/shard_map/all_to_all | solution.py:67
  124.9 0.6 reduce_sum.37
  125.5 1.4 broadcast_in_dim.24
  126.9 3.9 %all-to-all-start.3 = ((f32[16,1,14336]{2,1,0:T(1,128)}), f32[16,1,14336]{2,1,0:T(1,128)S(1)}, u32[]{:S(2)}, u32[]{:S(2)}) async-start(f32[16,1,14336]{2,1,0:T(1,128)} %broadcast_in_dim.24), calls=%async_computation.3 | async-start | bytes 1835008 | tf_op jit(solution)/shard_map/all_to_all | solution.py:19
  130.9 0.0 all-gather.2.cloned.1.call-start
  130.9 0.9 copy.51
  131.8 12.2 %all-to-all-done.3 = f32[16,1,14336]{2,1,0:T(1,128)S(1)} async-done(((f32[16,1,14336]{2,1,0:T(1,128)}), f32[16,1,14336]{2,1,0:T(1,128)S(1)}, u32[]{:S(2)}, u32[]{:S(2)}) %all-to-all-start.3) | async-done | bytes 917536 | tf_op jit(solution)/shard_map/all_to_all | solution.py:19
  144.1 0.1 slice.72
  144.1 0.2 reshape.79
  144.4 2.3 %multiply_reduce_fusion = (f32[]{:T(128)}, f32[3,256,256]{2,1,0:T(8,128)S(1)}, f32[3,256,256]{2,1,0:T(8,128)S(1)}) fusion(f32[3,256,256]{2,1,0:T(8,128)S(1)} %reshape.79, f32[3,256,256]{2,1,0:T(8,128)} %param.18, f32[3,256,256]{2,1,0:T(8,128)} %param.17), kind=kLoop, calls=%fused_computation.15 | loop fusion | flops 1966079 | bytes 3932164 | tf_op jit(solution)/shard_map/reduce_sum | solution.py:134
  146.6 0.7 broadcast_in_dim.25
  147.4 9.6 %all_to_all.36 = f32[8,1,1]{2,1,0:T(1,128)S(1)} all-to-all(f32[8,1,1]{2,1,0:T(1,128)S(1)} %broadcast_in_dim.25), channel_id=1, replica_groups=mesh['fs'=16,'tp'=8] {'tp'}, dimensions={0} | all-to-all | bytes 64 | tf_op jit(solution)/shard_map/all_to_all | solution.py:19
  156.9 0.6 reduce_sum.39
  158.3 2.7 %fusion.22 = (bf16[3,128,256]{1,2,0:T(8,128)(2,1)}, f32[3,128,256]{1,2,0:T(8,128)S(1)}, f32[3,128,256]{1,2,0:T(8,128)}) fusion(f32[3,128,256]{1,2,0:T(8,128)} %copy.51, bf16[3,128,256]{2,1,0:T(8,128)(2,1)S(1)} %copy-done.4, f32[3,256,256]{2,1,0:T(8,128)S(1)} %get-tuple-element.62, f32[3,256,256]{2,1,0:T(8,128)S(1)} %get-tuple-element.61, f32[]{:T(128)S(6)} %rsqrt.5), kind=kOutput, calls=%fused_computation.37 | convolution fusion | flops 302579712 | bytes 3145732 | tf_op jit(solution)/shard_map/rdk,rkw->rdw/dot_general | solution.py:137
  160.9 0.0 all-gather.2.cloned.1.call-update
  160.9 2.2 reduce.3
  163.1 0.1 slice.68
  163.3 1.7 fusion.20
  165.0 1.9 copy.52
  166.9 0.9 copy.53
  167.8 40.8 %all-gather.2.cloned.1.call-done = bf16[3,2048,256]{1,2,0:T(8,128)(2,1)} async-done(((bf16[3,128,256]{1,2,0:T(8,128)(2,1)}), bf16[3,2048,256]{1,2,0:T(8,128)(2,1)}) %all-gather.2.cloned.1.call-update) | async-done | bytes 3145744 | tf_op jit(solution)/shard_map/all_gather | solution.py:142
  208.7 4.6 %copy.54 = bf16[3,2048,256]{2,1,0:T(8,128)(2,1)} copy(bf16[3,2048,256]{1,2,0:T(8,128)(2,1)} %all-gather.2.cloned.1.call-done) | data formatting | bytes 6291456
  (32 shorter events, 0.2 us)
Async XLA Ops:
  8.8 15.5 %all-to-all-start.1 = ((f32[16,1,16]{2,1,0:T(1,128)}), f32[16,1,16]{2,1,0:T(1,128)S(1)}, u32[]{:S(2)}, u32[]{:S(2)}) async-start(f32[16,1,16]{2,1,0:T(1,128)} %broadcast_in_dim.22), calls=%async_computation.1 | async-start | bytes 16384 | tf_op jit(solution)/shard_map/all_to_all | solution.py:19
  17.9 12.6 %copy-start.2 = (f32[16,3072]{1,0:T(8,128)S(1)}, f32[16,3072]{1,0:T(8,128)}, u32[]{:S(2)}) copy-start(f32[16,3072]{1,0:T(8,128)} %param.13) | copy-start | bytes 589828
  18.0 17.5 %copy-start.3 = (f32[16,3072]{1,0:T(8,128)S(1)}, f32[16,3072]{1,0:T(8,128)}, u32[]{:S(2)}) copy-start(f32[16,3072]{1,0:T(8,128)} %param.14) | copy-start | bytes 589828
  24.4 2.4 %copy-start.8 = (f32[16,1,16]{2,1,0:T(1,128)}, f32[16,1,16]{2,1,0:T(1,128)S(1)}, u32[]{:S(2)}) copy-start(f32[16,1,16]{2,1,0:T(1,128)S(1)} %all-to-all-done.1) | copy-start | bytes 3076
  26.8 48.1 %all-to-all-start = ((bf16[16,3,128,256]{2,3,1,0:T(8,128)(2,1)}), bf16[16,3,128,256]{2,3,1,0:T(8,128)(2,1)S(1)}, u32[]{:S(2)}, u32[]{:S(2)}) async-start(bf16[16,3,128,256]{2,3,1,0:T(8,128)(2,1)} %stack.2), calls=%async_computation | async-start | bytes 6291456 | tf_op jit(solution)/shard_map/all_to_all | solution.py:119
  31.2 37.3 %collective-permute-start = (f32[16,1]{1,0:T(8,128)}, f32[16,1]{1,0:T(8,128)}, u32[]{:S(2)}, u32[]{:S(2)}) collective-permute-start(f32[16,1]{1,0:T(8,128)} %slice.65), channel_id=1, source_target_pairs={{0,8},{8,16},{16,24},{24,32},{32,40},{40,48},{48,56},{56,64},{64,7... | collective-permute-start | bytes 200 | tf_op jit(solution)/shard_map/ppermute | solution.py:14
  100.5 30.4 %copy-start.5 = (f32[3,128,256]{2,1,0:T(8,128)S(1)}, f32[3,128,256]{2,1,0:T(8,128)}, u32[]{:S(2)}) copy-start(f32[3,128,256]{2,1,0:T(8,128)} %param.15) | copy-start | bytes 1179652
  126.9 31.3 %copy-start.4 = (bf16[3,128,256]{2,1,0:T(8,128)(2,1)S(1)}, bf16[3,128,256]{2,1,0:T(8,128)(2,1)}, u32[]{:S(2)}) copy-start(bf16[3,128,256]{2,1,0:T(8,128)(2,1)} %param.16) | copy-start | bytes 589828
  126.9 17.2 %all-to-all-start.3 = ((f32[16,1,14336]{2,1,0:T(1,128)}), f32[16,1,14336]{2,1,0:T(1,128)S(1)}, u32[]{:S(2)}, u32[]{:S(2)}) async-start(f32[16,1,14336]{2,1,0:T(1,128)} %broadcast_in_dim.24), calls=%async_computation.3 | async-start | bytes 1835008 | tf_op jit(solution)/shard_map/all_to_all | solution.py:19
  130.9 77.8 %all-gather.2.cloned.1.call-start = ((), (), s32[]{:S(2)}) async-start(), calls=%async_computation.5 | async-start | bytes 3342336 | tf_op jit(solution)/shard_map/all_gather | solution.py:142
  146.6 14.3 %copy-start.1 = (f32[3,256,256]{2,1,0:T(8,128)}, f32[3,256,256]{2,1,0:T(8,128)S(1)}, u32[]{:S(2)}) copy-start(f32[3,256,256]{2,1,0:T(8,128)S(1)} %get-tuple-element.62) | copy-start | bytes 2359300
  146.6 21.2 %copy-start = (f32[3,256,256]{2,1,0:T(8,128)}, f32[3,256,256]{2,1,0:T(8,128)S(1)}, u32[]{:S(2)}) copy-start(f32[3,256,256]{2,1,0:T(8,128)S(1)} %get-tuple-element.61) | copy-start | bytes 2359300
  146.6 16.7 %copy-start.6 = (f32[16,2048]{1,0:T(8,128)S(1)}, f32[16,2048]{1,0:T(8,128)}, u32[]{:S(2)}) copy-start(f32[16,2048]{1,0:T(8,128)} %param.19) | copy-start | bytes 393220
  146.6 16.7 %copy-start.7 = (f32[16,2048]{1,0:T(8,128)S(1)}, f32[16,2048]{1,0:T(8,128)}, u32[]{:S(2)}) copy-start(f32[16,2048]{1,0:T(8,128)} %param.20) | copy-start | bytes 393220
Sparse Core Ops, SparseCore 0:
  161.1 47.5 all-gather.1
